TPU v7x, 32 devices: a whole 2x2x4 slice. The times are simulated.
32 devices in a mesh: sp: 8 (over z, y), tp: 4 (over x, core).
Axes of the slice: x: 2, y: 2, z: 4, core: 2. Of those that a mesh axis runs over, the one named last changes fastest.
Arguments:
- queries: bfloat16 [4096, 1024], P('sp', 'tp'), may hold values from -200 to 200
- keys: bfloat16 [4096, 1024], P('sp', 'tp'), may hold values from -6 to 6
- values: bfloat16 [4096, 1024], P('sp', 'tp'), may hold values from -24 to 24
- cum_gate: float32 [4096, 8], P('sp', 'tp'), may hold values from -414 to 0, as said below
- residual: bfloat16 [4096, 2048], P(('sp', 'tp')), may hold values from -1.5 to 1.5
- w_out: bfloat16 [1024, 2048], replicated, may hold values from -0.1875 to 0.1875
- gain: float32 [2048], replicated, may hold values from 0.1 to 1.9
- w_up: bfloat16 [2048, 8192], P('sp', 'tp'), may hold values from -0.125 to 0.125
- w_down: bfloat16 [8192, 2048], P('tp', 'sp'), may hold values from -0.0625 to 0.0625
Outputs:
- output: bfloat16 [4096, 2048], P(('sp', 'tp'))
Inputs may be any that keep to these rules, and one draw needn't show every extreme that they name: Within each head, cum_gate never rises from one position to the next.
All inputs are finite; a program needn't handle non-finite values.
Results may differ from a plain program's by a relative error of at most 0.022.
Values may be sent and summed in bfloat16 or wider, within the bound.
A program may use at most 128 MiB of HBM per device.

v0:
```python
import math

import jax
import jax.numpy as jnp
from jax import lax
from jax.sharding import PartitionSpec as P


def per_device(queries, keys, values, cum_gate, residual, w_out, gain, w_up, w_down):
    tok_rows, width = queries.shape
    heads_here = cum_gate.shape[1]
    head_size = width // heads_here
    score_scale = head_size ** (-0.5)
    row_offset = lax.axis_index("sp") * tok_rows
    query_heads = queries.reshape(tok_rows, heads_here, head_size)
    query_pos = row_offset + jnp.arange(tok_rows, dtype=jnp.int32)
    all_gates = lax.all_gather(cum_gate, "sp", axis=0, tiled=True)
    initial = (
        jnp.full((tok_rows, heads_here), -1e30, jnp.float32),
        jnp.zeros((tok_rows, heads_here), jnp.float32),
        jnp.zeros((tok_rows, heads_here, head_size), jnp.float32),
    )
    carried = initial
    key_rows = lax.all_gather(keys, "sp", axis=0, tiled=True)
    value_rows = lax.all_gather(values, "sp", axis=0, tiled=True)
    row_count = key_rows.shape[0]
    span_rows = math.gcd(row_count, 2048)
    block_count = row_count // span_rows
    key_blocks = key_rows.reshape(block_count, span_rows, heads_here, head_size)
    value_blocks = value_rows.reshape(block_count, span_rows, heads_here, head_size)
    first_pos = jnp.arange(block_count, dtype=jnp.int32) * span_rows

    def absorb_block(running, packed):
        running_max, running_sum, accumulated = running
        key_blk, value_blk, block_start = packed
        gate_blk = lax.dynamic_slice_in_dim(all_gates, block_start, span_rows, 0)
        scores = jnp.einsum(
            "qhd,khd->qhk", query_heads, key_blk, preferred_element_type=jnp.float32
        )
        scores = scores * score_scale + cum_gate[:, :, None] - gate_blk.T[None, :, :]
        key_pos = block_start + jnp.arange(span_rows, dtype=jnp.int32)
        scores = jnp.where(key_pos[None, None, :] <= query_pos[:, None, None], scores, -1e30)
        new_max = jnp.maximum(running_max, jnp.max(scores, axis=-1))
        rescale = jnp.exp(running_max - new_max)
        weights = jnp.exp(scores - new_max[:, :, None])
        running_sum = running_sum * rescale + jnp.sum(weights, axis=-1)
        product = jnp.einsum(
            "qhk,khd->qhd",
            weights.astype(jnp.bfloat16),
            value_blk,
            preferred_element_type=jnp.float32,
        )
        accumulated = accumulated * rescale[:, :, None] + product
        return ((new_max, running_sum, accumulated), None)

    carried, _ = lax.scan(absorb_block, carried, (key_blocks, value_blocks, first_pos))
    running_max, running_sum, accumulated = carried
    attended = (accumulated / running_sum[:, :, None]).reshape(tok_rows, width).astype(jnp.bfloat16)
    mine = lax.all_to_all(attended, "tp", split_axis=0, concat_axis=1, tiled=True)
    projected = jnp.dot(mine, w_out, preferred_element_type=jnp.float32)
    residual_sum = residual.astype(jnp.float32) + projected
    mean_square = jnp.mean(residual_sum * residual_sum, axis=-1, keepdims=True)
    normed = (residual_sum * lax.rsqrt(mean_square + 1e-06) * gain).astype(jnp.bfloat16)
    normed_all = lax.all_gather(normed, "tp", axis=0, tiled=True)
    up_proj = jnp.dot(
        normed_all,
        lax.all_gather(w_up, "sp", axis=0, tiled=True),
        preferred_element_type=jnp.float32,
    )
    hidden = jnp.square(jax.nn.relu(up_proj)).astype(jnp.bfloat16)
    down_whole = lax.all_gather(w_down, "sp", axis=1, tiled=True)
    rounded = jnp.dot(hidden, down_whole, preferred_element_type=jnp.float32).astype(jnp.bfloat16)
    branch_out = lax.psum_scatter(
        lax.optimization_barrier(rounded).astype(jnp.float32).astype(jnp.bfloat16),
        "tp",
        scatter_dimension=0,
        tiled=True,
    ).astype(jnp.float32)
    return (residual_sum + branch_out).astype(jnp.bfloat16)


def solution(mesh):
    return jax.shard_map(
        per_device,
        mesh=mesh,
        in_specs=(
            P("sp", "tp"),
            P("sp", "tp"),
            P("sp", "tp"),
            P("sp", "tp"),
            P(("sp", "tp"), None),
            P(),
            P(),
            P("sp", "tp"),
            P("tp", "sp"),
        ),
        out_specs=P(("sp", "tp"), None),
        check_vma=False,
    )
```

profile of v0, /device:TPU:19, one launch (start us, length us, event | category | flops | bytes accessed | tf_op | source)
XLA Modules:
  0.0 499.2 jit_solution(15590965651173478988)
XLA Ops:
  6.5 0.7 all-gather.6.cloned.1.call-update
  7.3 0.0 all-gather.8.cloned.1.call-start
  7.3 0.7 all-gather.8.cloned.1.call-update
  8.0 0.0 all-gather.10.cloned.1.call-start
  8.1 1.1 copy.17
  9.2 0.2 copy.19
  9.4 21.0 %all_gather.19 = f32[4096,2]{0,1:T(2,128)S(1)} all-gather(f32[512,2]{0,1:T(2,128)} %param.14), channel_id=1, replica_groups=mesh['sp'=8,'tp'=4] {'sp'}, dimensions={0}, use_global_device_ids=true | all-gather | bytes 36864 | tf_op jit(solution)/shard_map/all_gather | solution.py:17
  30.4 28.1 %all-gather.6.cloned.1.call-done = bf16[4096,256]{1,0:T(8,128)(2,1)} async-done(((bf16[512,256]{1,0:T(8,128)(2,1)}), bf16[4096,256]{1,0:T(8,128)(2,1)}) %all-gather.6.cloned.1.call-update) | async-done | bytes 2097168 | tf_op jit(solution)/shard_map/all_gather | solution.py:24
  58.5 4.0 reshape.62
  62.5 45.8 %all-gather.8.cloned.1.call-done = bf16[4096,256]{1,0:T(8,128)(2,1)} async-done(((bf16[512,256]{1,0:T(8,128)(2,1)}), bf16[4096,256]{1,0:T(8,128)(2,1)}) %all-gather.8.cloned.1.call-update) | async-done | bytes 2097168 | tf_op jit(solution)/shard_map/all_gather | solution.py:25
  108.2 4.0 reshape.64
  112.2 45.9 %while.15 = (s32[]{:T(128)}, f32[512,2]{0,1:T(2,128)S(1)}, f32[512,2]{0,1:T(2,128)S(1)}, f32[512,2,128]{0,2,1:T(8,128)}, s32[2]{0:T(128)S(1)}, /*index=5*/bf16[2...) while((s32[]{:T(128)}, f32[512,2]{0,1:T(2,128)S(1)}, ...), condition=%wide.region_3.4_spmd.clone, body=%wide.region_0.3_spmd.clone.sunk | while | flops 1110842880 | bytes 39239884 | solution.py:56
  112.2 0.6 dynamic_slice.26
  114.5 0.1 dynamic-slice_bitcast_fusion.2
  114.6 0.6 iota_add_fusion.5
  115.2 0.8 broadcast_compare_fusion.2
  115.9 2.7 constant_dynamic-slice_fusion.3
  118.6 4.6 fusion.40
  123.2 4.8 fusion.42
  128.1 0.8 copy.34
  128.9 6.2 %fusion.44 = f32[512,2,128]{0,2,1:T(8,128)} fusion(f32[2,2048,512]{2,1,0:T(8,128)} %get-tuple-element.231, f32[512,2]{0,1:T(2,128)S(1)} %fusion.41, f32[2,2048]{1,0:T(2,128)S(1)} %dynamic-slice_bitcast_fusion.2, f32[512,2]{0,1:T(2,128)S(1)} %get-tuple-element.270, pred[512,2048]{0,1:T(8,128)(4,1)S(1)} %broadcast_compare_fusion.2, ...), kind=kOutput, calls=%fused_computation.12.clone.1 | convolution fusion | flops 549847040 | bytes 11563009 | tf_op jit(solution)/shard_map/while/body/eval_jaxpr/qhk,khd->qhd/dot_general | solution.py:47
  135.1 0.6 dynamic_slice.26
  137.4 0.1 dynamic-slice_bitcast_fusion.2
  137.5 0.6 iota_add_fusion.5
  138.1 0.8 broadcast_compare_fusion.2
  138.8 2.7 constant_dynamic-slice_fusion.3
  141.5 4.6 fusion.40
  146.1 4.8 fusion.42
  150.9 0.8 copy.34
  151.8 6.4 %fusion.44 = f32[512,2,128]{0,2,1:T(8,128)} fusion(f32[2,2048,512]{2,1,0:T(8,128)} %get-tuple-element.231, f32[512,2]{0,1:T(2,128)S(1)} %fusion.41, f32[2,2048]{1,0:T(2,128)S(1)} %dynamic-slice_bitcast_fusion.2, f32[512,2]{0,1:T(2,128)S(1)} %get-tuple-element.270, pred[512,2048]{0,1:T(8,128)(4,1)S(1)} %broadcast_compare_fusion.2, ...), kind=kOutput, calls=%fused_computation.12.clone.1 | convolution fusion | flops 549847040 | bytes 11563009 | tf_op jit(solution)/shard_map/while/body/eval_jaxpr/qhk,khd->qhd/dot_general | solution.py:47
  158.1 1.1 divide_convert_fusion
  159.2 0.1 reshape.65
  159.3 0.2 copy.24
  159.5 8.3 %all_to_all.16 = bf16[4,128,256]{2,1,0:T(8,128)(2,1)S(1)} all-to-all(bf16[4,128,256]{2,1,0:T(8,128)(2,1)S(1)} %copy.24), channel_id=1, replica_groups=mesh['sp'=8,'tp'=4] {'tp'}, dimensions={0} | all-to-all | bytes 524288 | tf_op jit(solution)/shard_map/all_to_all | solution.py:59
  167.8 0.2 copy.22
  167.9 3.1 multiply_reduce_fusion
  171.1 0.9 multiply_convert_fusion.1
  172.1 0.0 all-gather.12.cloned.1.call-start
  172.1 0.5 all-gather.12.cloned.1.call-update
  172.6 0.0 all-gather.14.cloned.1.call-start
  172.7 0.5 all-gather.14.cloned.1.call-update
  173.2 0.2 reduce-scatter.2.cloned.1.call-start
  173.5 20.0 %all-gather.10.cloned.1.call-done = bf16[512,2048]{1,0:T(8,128)(2,1)} async-done(((bf16[128,2048]{1,0:T(8,128)(2,1)}), bf16[512,2048]{1,0:T(8,128)(2,1)}) %all-gather.10.cloned.1.call-update) | async-done | bytes 2097168 | tf_op jit(solution)/shard_map/all_gather | solution.py:64
  193.4 125.4 %all-gather.12.cloned.1.call-done = bf16[2048,2048]{1,0:T(8,128)(2,1)} async-done(((bf16[256,2048]{1,0:T(8,128)(2,1)}), bf16[2048,2048]{1,0:T(8,128)(2,1)}) %all-gather.12.cloned.1.call-update) | async-done | bytes 8388624 | tf_op jit(solution)/shard_map/all_gather | solution.py:67
  318.8 125.0 %all-gather.14.cloned.1.call-done = bf16[2048,2048]{1,0:T(8,128)(2,1)} async-done(((bf16[2048,256]{1,0:T(8,128)(2,1)}), bf16[2048,2048]{1,0:T(8,128)(2,1)}) %all-gather.14.cloned.1.call-update) | async-done | bytes 8388624 | tf_op jit(solution)/shard_map/all_gather | solution.py:71
  443.8 16.5 %convolution_convert_fusion = bf16[512,2048]{1,0:T(8,128)(2,1)} fusion(bf16[2048,2048]{1,0:T(8,128)(2,1)} %all-gather.14.cloned.1.call-done, bf16[512,2048]{1,0:T(8,128)(2,1)} %all-gather.10.cloned.1.call-done, bf16[2048,2048]{1,0:T(8,128)(2,1)} %all-gather.12.cloned.1.call-done), kind=kOutput, calls=%fused_computation.30 | convolution fusion | flops 8594128896 | bytes 20971520 | tf_op jit(solution)/shard_map/dot_general | solution.py:72
  460.4 30.0 %reduce-scatter.2.cloned.1.call-done = bf16[128,2048]{1,0:T(8,128)(2,1)} async-done(((bf16[512,2048]{1,0:T(8,128)(2,1)}), bf16[128,2048]{1,0:T(8,128)(2,1)}) %reduce-scatter.2.cloned.1.call-update) | async-done | bytes 524304 | tf_op jit(solution)/shard_map/reduce_scatter | solution.py:73
  490.4 1.9 add_convert_fusion
  (20 shorter events, 0.1 us)
Async XLA Ops:
  6.5 105.7 %copy-start = (f32[512,2]{0,1:T(2,128)S(1)}, f32[512,2]{0,1:T(2,128)}, u32[]{:S(2)}) copy-start(f32[512,2]{0,1:T(2,128)} %param.14) | copy-start | bytes 12292
  6.5 51.9 %all-gather.6.cloned.1.call-start = ((), (), s32[]{:S(2)}) async-start(), calls=%async_computation.2 | async-start | bytes 2359296 | tf_op jit(solution)/shard_map/all_gather | solution.py:24
  7.3 101.0 %all-gather.8.cloned.1.call-start = ((), (), s32[]{:S(2)}) async-start(), calls=%async_computation.3 | async-start | bytes 2359296 | tf_op jit(solution)/shard_map/all_gather | solution.py:25
  8.0 185.4 %all-gather.10.cloned.1.call-start = ((), (), s32[]{:S(2)}) async-start(), calls=%async_computation.4 | async-start | bytes 2621440 | tf_op jit(solution)/shard_map/all_gather | solution.py:64
  158.1 13.0 %copy-start.1 = (f32[2048]{0:T(1024)S(1)}, f32[2048]{0:T(1024)}, u32[]{:S(2)}) copy-start(f32[2048]{0:T(1024)} %param.17) | copy-start | bytes 24580
  172.1 146.7 %all-gather.12.cloned.1.call-start = ((), (), s32[]{:S(2)}) async-start(), calls=%async_computation.5 | async-start | bytes 9437184 | tf_op jit(solution)/shard_map/all_gather | solution.py:67
  172.6 271.2 %all-gather.14.cloned.1.call-start = ((), (), s32[]{:S(2)}) async-start(), calls=%async_computation.6 | async-start | bytes 9437184 | tf_op jit(solution)/shard_map/all_gather | solution.py:71
  173.2 317.2 %reduce-scatter.2.cloned.1.call-start = ((), (), s32[]{:S(2)}) async-start(), calls=%async_computation.7 | async-start | bytes 2621440 | tf_op jit(solution)/shard_map/reduce_scatter | solution.py:73
Sparse Core Ops, SparseCore 0:
  9.5 48.9 all-gather.5
  60.6 47.6 all-gather.7
  172.2 21.1 all-gather.9
  195.4 123.3 all-gather.11
  320.7 123.1 all-gather.13
  460.5 29.8 reduce-scatter.1
where the time goes:
time: 502 us; the launch traced here: 499 us
  waiting for transfers between devices  377 us (75%)
  matrix products  41.5 us (8%)
  blocking collectives  29.3 us (6%)
  local copies, waits for them, and re-layouts  18 us (4%)
  other arithmetic  16.3 us (3%)
  between operations  13.6 us (3%)
    all_gather x1, waiting for transfers between devices, per_device(): lax.all_gather(w_up, 'sp', axis=0, tiled=True)  125 us
    all_gather x1, waiting for transfers between devices, per_device(): down_whole = lax.all_gather(w_down, 'sp', axis=1, tiled=True)  125 us
    all_gather x1, waiting for transfers between devices, per_device(): value_rows = lax.all_gather(values, 'sp', axis=0, tiled=True)  45.8 us
    reduce_scatter x1, waiting for transfers between devices, per_device(): lax.psum_scatter(lax.optimization_barrier(rounded).astype(jnp.float32).as...  30 us
    all_gather x1, waiting for transfers between devices, per_device(): key_rows = lax.all_gather(keys, 'sp', axis=0, tiled=True)  28.1 us
    all_gather x1, blocking collectives, per_device(): all_gates = lax.all_gather(cum_gate, 'sp', axis=0, tiled=True)  21 us
    all_gather x1, waiting for transfers between devices, per_device(): normed_all = lax.all_gather(normed, 'tp', axis=0, tiled=True)  20 us
    dot_general x1, matrix products, per_device(): jnp.dot(hidden, down_whole, preferred_element_type=jnp.float32)  16.5 us
  transfers between devices with their start and end apart: 6, of which 6 were waited for; matrix products, arithmetic and copies ran while one was open for 1% of the time, Pallas kernels for 0%

commit v1 on v0

v1 whole, which is shorter than its diff:
```python
import functools
import math

import jax
import jax.numpy as jnp
from jax import lax
from jax.experimental import pallas as pl
from jax.experimental.pallas import tpu as pltpu
from jax.sharding import PartitionSpec as P

LOG2E = math.log2(math.e)
NEG = -1e30


def body(
    n_sp, n_tp, heads,
    q_ref, kv_ref, gate_ref, res_ref, wout_hbm, gain_ref, wup_hbm, wdn_hbm,
    out_ref,
    kv_all, gate_all, m_s, l_s, acc_s, att, att_in, wout, rsum,
    wu, wd, norm_all, hid, psend, precv,
    kv_s1, kv_s2, kv_r, g_s1, g_s2, g_r, u_s1, u_s2, u_r, d_s1, d_s2, d_r,
    a_s, a_r, n_s, n_r, p_s, p_r, loc,
):
    ny = n_tp // 2
    nz = n_sp // ny
    tok, width = q_ref.shape
    hd = width // heads
    rows = tok // n_tp
    group = 2 * n_tp
    half = wu.shape[1]
    up_rows = wup_hbm.shape[0]
    features = res_ref.shape[1]
    cs = wdn_hbm.shape[1]
    me = lax.axis_index("sp")
    tp = lax.axis_index("tp")
    z, y = me // ny, me % ny
    par = z % 2
    slot = par * n_tp + tp

    def rcopy(src, dst, ss, rs, sp_to, tp_to=None):
        where = {"sp": sp_to} if tp_to is None else {"sp": sp_to, "tp": tp_to}
        return pltpu.make_async_remote_copy(
            src_ref=src, dst_ref=dst, send_sem=ss, recv_sem=rs,
            device_id=where, device_id_type=pl.DeviceIdType.MESH,
        )

    def member(o):
        other = (slot + o) % group
        return other, (z - par + other // n_tp) * ny + y, other % n_tp

    barrier = pltpu.get_barrier_semaphore()
    for dz in range(1, nz):
        pl.semaphore_signal(barrier, inc=1, device_id={"sp": ((z + dz) % nz) * ny + y},
                            device_id_type=pl.DeviceIdType.MESH)
    for dy in range(1, ny):
        pl.semaphore_signal(barrier, inc=1, device_id={"sp": z * ny + (y + dy) % ny},
                            device_id_type=pl.DeviceIdType.MESH)
    for o in range(1, group):
        _, sp_to, tp_to = member(o)
        pl.semaphore_signal(barrier, inc=1, device_id={"sp": sp_to, "tp": tp_to},
                            device_id_type=pl.DeviceIdType.MESH)
    pl.semaphore_wait(barrier, nz - 1 + ny - 1 + group - 1)

    def kv_first(dz):
        to = (z + dz) * ny + y
        return (rcopy(kv_ref, kv_all.at[me], kv_s1.at[dz], kv_r.at[me], to),
                rcopy(gate_ref, gate_all.at[me], g_s1.at[dz], g_r.at[me], to))

    def kv_own(dy):
        to = z * ny + (y + dy) % ny
        return (rcopy(kv_ref, kv_all.at[me], kv_s2.at[z * ny + dy], kv_r.at[me], to),
                rcopy(gate_ref, gate_all.at[me], g_s2.at[z * ny + dy], g_r.at[me], to))

    def kv_forward(zs, dy):
        s = zs * ny + y
        to = z * ny + (y + dy) % ny
        return (rcopy(kv_all.at[s], kv_all.at[s], kv_s2.at[zs * ny + dy], kv_r.at[s], to),
                rcopy(gate_all.at[s], gate_all.at[s], g_s2.at[zs * ny + dy], g_r.at[s], to))

    def wu_at(s):
        return wu.at[pl.ds(pl.multiple_of(s * up_rows, up_rows), up_rows), :]

    def up_half(p):
        return wup_hbm.at[:, pl.ds(pl.multiple_of(p * half, half), half)]

    def dn_half(p):
        return wdn_hbm.at[pl.ds(pl.multiple_of(p * half, half), half), :]

    def up_first(dz):
        zt = (z + dz) % nz
        return rcopy(up_half(zt % 2), wu_at(me), u_s1.at[dz], u_r.at[me], zt * ny + y)

    def dn_first(dz):
        zt = (z + dz) % nz
        return rcopy(dn_half(zt % 2), wd.at[me], d_s1.at[dz], d_r.at[me], zt * ny + y)

    def up_own(dy):
        return rcopy(up_half(par), wu_at(me), u_s2.at[z * ny + dy], u_r.at[me], z * ny + (y + dy) % ny)

    def dn_own(dy):
        return rcopy(dn_half(par), wd.at[me], d_s2.at[z * ny + dy], d_r.at[me], z * ny + (y + dy) % ny)

    def up_forward(zs, dy):
        s = zs * ny + y
        return rcopy(wu_at(s), wu_at(s), u_s2.at[zs * ny + dy], u_r.at[s], z * ny + (y + dy) % ny)

    def dn_forward(zs, dy):
        s = zs * ny + y
        return rcopy(wd.at[s], wd.at[s], d_s2.at[zs * ny + dy], d_r.at[s], z * ny + (y + dy) % ny)

    for dz in range(1, nz):
        @pl.when(z + dz < nz)
        def _(dz=dz):
            for c in kv_first(dz):
                c.start()
    for dy in range(1, ny):
        @pl.when((y + dy) % ny > y)
        def _(dy=dy):
            for c in kv_own(dy):
                c.start()
    local_wout = pltpu.make_async_copy(wout_hbm, wout, loc.at[0])
    local_up = pltpu.make_async_copy(up_half(par), wu_at(me), loc.at[1])
    local_dn = pltpu.make_async_copy(dn_half(par), wd.at[me], loc.at[2])
    local_wout.start()
    local_up.start()
    local_dn.start()
    for dz in range(1, nz):
        up_first(dz).start()
    for dy in range(1, ny):
        up_own(dy).start()
    for dz in range(1, nz):
        dn_first(dz).start()
    for dy in range(1, ny):
        dn_own(dy).start()

    scale = hd ** (-0.5) * LOG2E

    def absorb(kv, gates, diagonal):
        for h in range(heads):
            cols = pl.ds(h * hd, hd)
            rel = (gates[h:h + 1, :] - gate_ref[h:h + 1, 0:1]) * LOG2E
            s = lax.dot_general(q_ref[:, cols], kv[:, cols], (((1,), (1,)), ((), ())),
                                preferred_element_type=jnp.float32)
            s = s * scale - rel
            if diagonal:
                qp = lax.broadcasted_iota(jnp.int32, s.shape, 0)
                kp = lax.broadcasted_iota(jnp.int32, s.shape, 1)
                s = jnp.where(kp <= qp, s, NEG)
            top = jnp.max(s, axis=1, keepdims=True)
            if not diagonal:
                old = m_s[:, h:h + 1]
                top = jnp.maximum(old, top)
                fade = jnp.exp2(old - top)
            w = jnp.exp2(s - top)
            total = jnp.sum(w, axis=1, keepdims=True)
            add = jnp.dot(w.astype(jnp.bfloat16), kv[:, pl.ds(width + h * hd, hd)],
                          preferred_element_type=jnp.float32)
            if not diagonal:
                total = l_s[:, h:h + 1] * fade + total
                add = acc_s[:, cols] * fade + add
            m_s[:, h:h + 1] = top
            l_s[:, h:h + 1] = total
            acc_s[:, cols] = add

    absorb(kv_ref, gate_ref, True)

    def level(i, carry):
        zs = z - i

        @pl.when(zs >= 0)
        def _():
            @pl.when(i > 0)
            def _():
                own = zs * ny + y
                rcopy(kv_ref, kv_all.at[own], kv_s1.at[0], kv_r.at[own], me).wait_recv()
                rcopy(gate_ref, gate_all.at[own], g_s1.at[0], g_r.at[own], me).wait_recv()
                for dy in range(1, ny):
                    for c in kv_forward(zs, dy):
                        c.start()

            def column(dy, carry):
                s = zs * ny + (y + dy) % ny

                @pl.when(s < me)
                def _():
                    @pl.when(dy > 0)
                    def _():
                        rcopy(kv_ref, kv_all.at[s], kv_s1.at[0], kv_r.at[s], me).wait_recv()
                        rcopy(gate_ref, gate_all.at[s], g_s1.at[0], g_r.at[s], me).wait_recv()
                    absorb(kv_all.at[s], gate_all.at[s], False)
                return carry

            lax.fori_loop(0, ny, column, 0)
        return carry

    lax.fori_loop(0, nz, level, 0)

    for h in range(heads):
        cols = pl.ds(h * hd, hd)
        done = (acc_s[:, cols] / l_s[:, h:h + 1]).astype(jnp.bfloat16)
        for j in range(n_tp):
            att[j, :, cols] = done[j * rows:(j + 1) * rows, :]

    def heads_to(o):
        to = (tp + o) % n_tp
        return rcopy(att.at[to], att_in.at[tp], a_s.at[o], a_r.at[tp], me, to)

    for o in range(1, n_tp):
        heads_to(o).start()
    att_in[pl.ds(tp, 1)] = att[pl.ds(tp, 1)]
    local_wout.wait()
    for o in range(1, n_tp):
        src = (tp + o) % n_tp
        rcopy(att.at[0], att_in.at[src], a_s.at[0], a_r.at[src], me, tp).wait_recv()
    total = res_ref[...].astype(jnp.float32)
    for j in range(n_tp):
        total += jnp.dot(att_in[j], wout[j * width:(j + 1) * width, :], preferred_element_type=jnp.float32)
    rsum[...] = total
    mean_square = jnp.mean(total * total, axis=-1, keepdims=True)
    normed = (total * lax.rsqrt(mean_square + 1e-06) * gain_ref[...]).astype(jnp.bfloat16)

    def block(ref, b):
        return ref.at[pl.ds(pl.multiple_of(b * rows, rows), rows), :]

    block(norm_all, slot)[...] = normed

    def normed_to(o):
        _, sp_to, tp_to = member(o)
        return rcopy(block(norm_all, slot), block(norm_all, slot), n_s.at[o], n_r.at[slot], sp_to, tp_to)

    for o in range(1, group):
        normed_to(o).start()

    for dz in range(1, nz):
        zs = (z - dz + nz) % nz
        s = zs * ny + y
        rcopy(up_half(0), wu_at(s), u_s1.at[0], u_r.at[s], me).wait_recv()
        for dy in range(1, ny):
            up_forward(zs, dy).start()
    for dz in range(1, nz):
        zs = (z - dz + nz) % nz
        s = zs * ny + y
        rcopy(dn_half(0), wd.at[s], d_s1.at[0], d_r.at[s], me).wait_recv()
        for dy in range(1, ny):
            dn_forward(zs, dy).start()
    local_up.wait()
    local_dn.wait()
    for dy in range(1, ny):
        for zs in range(nz):
            s = zs * ny + (y + dy) % ny
            rcopy(up_half(0), wu_at(s), u_s1.at[0], u_r.at[s], me).wait_recv()
    for o in range(1, group):
        src = (slot + o) % group
        rcopy(block(norm_all, src), block(norm_all, src), n_s.at[0], n_r.at[src], me).wait_recv()

    tile = min(256, half)

    def up_tile(i, carry):
        cols = pl.ds(pl.multiple_of(i * tile, tile), tile)
        u = jnp.maximum(jnp.dot(norm_all[...], wu[:, cols], preferred_element_type=jnp.float32), 0.0)
        hid[:, cols] = (u * u).astype(jnp.bfloat16)
        return carry

    lax.fori_loop(0, half // tile, up_tile, 0)
    for dy in range(1, ny):
        for zs in range(nz):
            s = zs * ny + (y + dy) % ny
            rcopy(dn_half(0), wd.at[s], d_s1.at[0], d_r.at[s], me).wait_recv()

    per = max(1, 128 // cs)

    def dn_tile(i, carry):
        if per == 1:
            w = wd[i]
        else:
            w = jnp.concatenate([wd[i * per + k] for k in range(per)], axis=1)
        cols = pl.ds(pl.multiple_of(i * per * cs, per * cs), per * cs)
        psend[:, cols] = jnp.dot(hid[...], w, preferred_element_type=jnp.float32).astype(jnp.bfloat16)
        return carry

    lax.fori_loop(0, features // (per * cs), dn_tile, 0)

    def partial_to(o):
        other, sp_to, tp_to = member(o)
        return rcopy(block(psend, other), block(precv, slot), p_s.at[o], p_r.at[slot], sp_to, tp_to)

    for o in range(1, group):
        partial_to(o).start()
    total = rsum[...] + block(psend, slot)[...].astype(jnp.float32)
    for o in range(1, group):
        src = (slot + o) % group
        rcopy(block(psend, src), block(precv, src), p_s.at[0], p_r.at[src], me).wait_recv()
        total += block(precv, src)[...].astype(jnp.float32)
    out_ref[...] = total.astype(jnp.bfloat16)

    for dz in range(1, nz):
        @pl.when(z + dz < nz)
        def _(dz=dz):
            for c in kv_first(dz):
                c.wait_send()
        up_first(dz).wait_send()
        dn_first(dz).wait_send()
    for dy in range(1, ny):
        @pl.when((y + dy) % ny > y)
        def _(dy=dy):
            for c in kv_own(dy):
                c.wait_send()
        up_own(dy).wait_send()
        dn_own(dy).wait_send()
        for dz in range(1, nz):
            zs = (z - dz + nz) % nz

            @pl.when(z - dz >= 0)
            def _(zs=zs, dy=dy):
                for c in kv_forward(zs, dy):
                    c.wait_send()
            up_forward(zs, dy).wait_send()
            dn_forward(zs, dy).wait_send()
    for o in range(1, n_tp):
        heads_to(o).wait_send()
    for o in range(1, group):
        normed_to(o).wait_send()
        partial_to(o).wait_send()


def per_device(n_sp, n_tp, queries, keys, values, cum_gate, residual, w_out, gain, w_up, w_down):
    tok, width = queries.shape
    heads = cum_gate.shape[1]
    rows, features = residual.shape
    ny = n_tp // 2
    nz = n_sp // ny
    group = 2 * n_tp
    half = w_up.shape[1] // 2
    bf, f32 = jnp.bfloat16, jnp.float32
    gates = jnp.pad(cum_gate.T, ((0, 8 - heads), (0, 0)))
    kv = jnp.concatenate([keys, values], axis=1)
    vmem = pl.BlockSpec(memory_space=pltpu.VMEM)
    hbm = pl.BlockSpec(memory_space=pl.ANY)
    dma = lambda n: pltpu.SemaphoreType.DMA((n,))
    return pl.pallas_call(
        functools.partial(body, n_sp, n_tp, heads),
        out_shape=jax.ShapeDtypeStruct((rows, features), bf),
        in_specs=[vmem, vmem, vmem, vmem, hbm, vmem, hbm, hbm],
        out_specs=vmem,
        scratch_shapes=[
            pltpu.VMEM((n_sp, tok, 2 * width), bf),
            pltpu.VMEM((n_sp,) + gates.shape, f32),
            pltpu.VMEM((tok, 128), f32),
            pltpu.VMEM((tok, 128), f32),
            pltpu.VMEM((tok, width), f32),
            pltpu.VMEM((n_tp, rows, width), bf),
            pltpu.VMEM((n_tp, rows, width), bf),
            pltpu.VMEM(w_out.shape, bf),
            pltpu.VMEM((rows, features), f32),
            pltpu.VMEM((n_sp * w_up.shape[0], half), bf),
            pltpu.VMEM((n_sp, half, w_down.shape[1]), bf),
            pltpu.VMEM((group * rows, features), bf),
            pltpu.VMEM((group * rows, half), bf),
            pltpu.VMEM((group * rows, features), bf),
            pltpu.VMEM((group * rows, features), bf),
        ]
        + [dma(nz), dma(n_sp), dma(n_sp)] * 4
        + [dma(n_tp), dma(n_tp), dma(group), dma(group), dma(group), dma(group), dma(3)],
        compiler_params=pltpu.CompilerParams(
            collective_id=0, has_side_effects=True, vmem_limit_bytes=63 * 1024 * 1024
        ),
    )(queries, kv, gates, residual, w_out, gain.reshape(1, -1), w_up, w_down)


def solution(mesh):
    n_sp, n_tp = mesh.shape["sp"], mesh.shape["tp"]
    return jax.shard_map(
        functools.partial(per_device, n_sp, n_tp),
        mesh=mesh,
        in_specs=(
            P("sp", "tp"),
            P("sp", "tp"),
            P("sp", "tp"),
            P("sp", "tp"),
            P(("sp", "tp"), None),
            P(),
            P(),
            P("sp", "tp"),
            P("tp", "sp"),
        ),
        out_specs=P(("sp", "tp"), None),
        check_vma=False,
    )
```

time: 502 us -> 235 us (0.47)
  waiting for transfers between devices: 377 us -> 0 us
  Pallas kernels: 0 us -> 229 us
  matrix products: 41.5 us -> 0 us
  blocking collectives: 29.3 us -> 0 us
  local copies, waits for them, and re-layouts: 18 us -> 3.17 us
  other arithmetic: 16.3 us -> 1.86 us
  between operations: 13.6 us -> 0.01 us
    all_gather x5 -> x0, waiting for transfers between devices: 344 us -> none  [the longest x1 125 us: per_device(): lax.all_gather(w_up, 'sp', axis=0, tiled=True)]
    pallas_call x0 -> x1, Pallas kernels: none -> 229 us  [per_device(): pl.pallas_call(functools.partial(body, n_sp, n_tp, heads), out_shape=jax....]
    dot_general x6 -> x0, matrix products: 41.5 us -> none  [the longest x1 16.5 us: per_device(): jnp.dot(hidden, down_whole, preferred_element_type=jnp.float32)]
    reduce_scatter x1 -> x0, waiting for transfers between devices: 30 us -> none  [per_device(): lax.psum_scatter(lax.optimization_barrier(rounded).astype(jnp.float32).as...]
    all_gather x1 -> x0, blocking collectives: 21 us -> none  [per_device(): all_gates = lax.all_gather(cum_gate, 'sp', axis=0, tiled=True)]
    reduce_sum x2 -> x0, other arithmetic: 9.55 us -> none  [absorb_block(): running_sum = running_sum * rescale + jnp.sum(weights, axis=-1)]
    all_to_all x1 -> x0, blocking collectives: 8.29 us -> none  [per_device(): lax.all_to_all(attended, 'tp', split_axis=0, concat_axis=1, tiled=True)]
    dynamic_slice x6 -> x0, local copies, waits for them, and re-layouts: 8.16 us -> none  [per_device(): lax.scan(absorb_block, carried, (key_blocks, value_blocks, first_pos))]
  transfers between devices with their start and end apart: 6 -> 0, of which waited for: 6 -> 0; matrix products, arithmetic and copies ran while one was open for 1% -> 0% of each run, Pallas kernels for 0% -> 0%
where the time goes in v1:
time: 235 us; the launch traced here: 234 us
  Pallas kernels  229 us (97%)
  local copies, waits for them, and re-layouts  3.17 us (1%)
    pallas_call x1, Pallas kernels, per_device(): pl.pallas_call(functools.partial(body, n_sp, n_tp, heads), out_shape=jax....  229 us

profile of v1, /device:TPU:19, one launch (start us, length us, event | category | flops | bytes accessed | tf_op | source)
XLA Modules:
  0.0 234.3 jit_solution(16853685224929314075)
XLA Ops:
  0.0 1.3 pad.4.gate_ref
  1.3 1.9 pad_maximum_fusion.kv_ref
  3.1 229.3 %shard_map.91 = bf16[128,2048]{1,0:T(8,128)(2,1)} custom-call(bf16[512,256]{1,0:T(8,128)(2,1)} %q_ref.1, bf16[512,512]{1,0:T(8,128)(2,1)} %pad_maximum_fusion.kv_ref, f32[8,512]{1,0:T(8,128)} %pad.4.gate_ref, bf16[128,2048]{1,0:T(8,128)(2,1)} %res_ref.1, bf16[1024,2048]{1,0:T(8,128)(2,1)} %wout_hbm.1, f32[1,2048]{1,0:T(1,128)} %bitcast.2, ...), custom_call_target="tpu_custom_call" | custom-call | tf_op jit(solution)/shard_map/pallas_call | solution.py:340
  232.4 1.9 copy.11

commit v2 on v1

--- a/solution.py
+++ b/solution.py
@@ -128,10 +128,6 @@
         up_first(dz).start()
     for dy in range(1, ny):
         up_own(dy).start()
-    for dz in range(1, nz):
-        dn_first(dz).start()
-    for dy in range(1, ny):
-        dn_own(dy).start()
 
     scale = hd ** (-0.5) * LOG2E
 
@@ -224,12 +220,28 @@
 
     block(norm_all, slot)[...] = normed
 
-    def normed_to(o):
-        _, sp_to, tp_to = member(o)
-        return rcopy(block(norm_all, slot), block(norm_all, slot), n_s.at[o], n_r.at[slot], sp_to, tp_to)
-
-    for o in range(1, group):
-        normed_to(o).start()
+    def normed_row(src, sem, other):
+        zo, to = other // n_tp, other % n_tp
+        return rcopy(block(norm_all, src), block(norm_all, src), n_s.at[sem], n_r.at[src],
+                     (z - par + zo) * ny + y, to)
+
+    chips = group // 2
+    core = tp % 2
+    mate = slot + 1 - 2 * core
+
+    def normed_chip(k):
+        return normed_row(slot, k, (slot + 2 * k) % group)
+
+    def normed_mate(k):
+        return normed_row((slot + 2 * k) % group, chips + k, mate)
+
+    for k in range(1, chips):
+        normed_chip(k).start()
+    normed_mate(0).start()
+    for dz in range(1, nz):
+        dn_first(dz).start()
+    for dy in range(1, ny):
+        dn_own(dy).start()
 
     for dz in range(1, nz):
         zs = (z - dz + nz) % nz
@@ -237,20 +249,25 @@
         rcopy(up_half(0), wu_at(s), u_s1.at[0], u_r.at[s], me).wait_recv()
         for dy in range(1, ny):
             up_forward(zs, dy).start()
-    for dz in range(1, nz):
+    for k in range(1, chips):
+        src = (slot + 2 * k) % group
+        rcopy(block(norm_all, src), block(norm_all, src), n_s.at[0], n_r.at[src], me).wait_recv()
+        normed_mate(k).start()
+
+    def down_on(dz):
         zs = (z - dz + nz) % nz
         s = zs * ny + y
         rcopy(dn_half(0), wd.at[s], d_s1.at[0], d_r.at[s], me).wait_recv()
         for dy in range(1, ny):
             dn_forward(zs, dy).start()
+
     local_up.wait()
-    local_dn.wait()
     for dy in range(1, ny):
         for zs in range(nz):
             s = zs * ny + (y + dy) % ny
             rcopy(up_half(0), wu_at(s), u_s1.at[0], u_r.at[s], me).wait_recv()
-    for o in range(1, group):
-        src = (slot + o) % group
+    for k in range(chips):
+        src = (mate + 2 * k) % group
         rcopy(block(norm_all, src), block(norm_all, src), n_s.at[0], n_r.at[src], me).wait_recv()
 
     tile = min(256, half)
@@ -262,34 +279,44 @@
         return carry
 
     lax.fori_loop(0, half // tile, up_tile, 0)
-    for dy in range(1, ny):
-        for zs in range(nz):
+
+    per = max(1, 128 // cs)
+    span = ny * cs
+
+    def part(ref, b, zs):
+        return ref.at[pl.ds(pl.multiple_of(b * rows, rows), rows),
+                      pl.ds(pl.multiple_of(zs * span, span), span)]
+
+    def partial_to(o, zs):
+        other, sp_to, tp_to = member(o)
+        return rcopy(part(psend, other, zs), part(precv, slot, zs), p_s.at[o * nz + zs],
+                     p_r.at[slot * nz + zs], sp_to, tp_to)
+
+    def down_level(dz):
+        zs = (z - dz + nz) % nz
+        for k in range(ny // per):
+            ws = [wd[zs * ny + k * per + i] for i in range(per)]
+            w = ws[0] if per == 1 else jnp.concatenate(ws, axis=1)
+            cols = pl.ds(pl.multiple_of((zs * ny + k * per) * cs, per * cs), per * cs)
+            psend[:, cols] = jnp.dot(hid[...], w, preferred_element_type=jnp.float32).astype(jnp.bfloat16)
+        for o in range(1, group):
+            partial_to(o, zs).start()
+
+    local_dn.wait()
+    for dz in range(nz):
+        if dz + 1 < nz:
+            down_on(dz + 1)
+        zs = (z - dz + nz) % nz
+        for dy in range(1, ny):
             s = zs * ny + (y + dy) % ny
             rcopy(dn_half(0), wd.at[s], d_s1.at[0], d_r.at[s], me).wait_recv()
-
-    per = max(1, 128 // cs)
-
-    def dn_tile(i, carry):
-        if per == 1:
-            w = wd[i]
-        else:
-            w = jnp.concatenate([wd[i * per + k] for k in range(per)], axis=1)
-        cols = pl.ds(pl.multiple_of(i * per * cs, per * cs), per * cs)
-        psend[:, cols] = jnp.dot(hid[...], w, preferred_element_type=jnp.float32).astype(jnp.bfloat16)
-        return carry
-
-    lax.fori_loop(0, features // (per * cs), dn_tile, 0)
-
-    def partial_to(o):
-        other, sp_to, tp_to = member(o)
-        return rcopy(block(psend, other), block(precv, slot), p_s.at[o], p_r.at[slot], sp_to, tp_to)
-
-    for o in range(1, group):
-        partial_to(o).start()
+        down_level(dz)
+
     total = rsum[...] + block(psend, slot)[...].astype(jnp.float32)
     for o in range(1, group):
         src = (slot + o) % group
-        rcopy(block(psend, src), block(precv, src), p_s.at[0], p_r.at[src], me).wait_recv()
+        for zs in range(nz):
+            rcopy(part(psend, src, zs), part(precv, src, zs), p_s.at[0], p_r.at[src * nz + zs], me).wait_recv()
         total += block(precv, src)[...].astype(jnp.float32)
     out_ref[...] = total.astype(jnp.bfloat16)
 
@@ -318,9 +345,13 @@
             dn_forward(zs, dy).wait_send()
     for o in range(1, n_tp):
         heads_to(o).wait_send()
+    for k in range(1, chips):
+        normed_chip(k).wait_send()
+    for k in range(chips):
+        normed_mate(k).wait_send()
     for o in range(1, group):
-        normed_to(o).wait_send()
-        partial_to(o).wait_send()
+        for zs in range(nz):
+            partial_to(o, zs).wait_send()
 
 
 def per_device(n_sp, n_tp, queries, keys, values, cum_gate, residual, w_out, gain, w_up, w_down):
@@ -360,7 +391,7 @@
             pltpu.VMEM((group * rows, features), bf),
         ]
         + [dma(nz), dma(n_sp), dma(n_sp)] * 4
-        + [dma(n_tp), dma(n_tp), dma(group), dma(group), dma(group), dma(group), dma(3)],
+        + [dma(n_tp), dma(n_tp), dma(group), dma(group), dma(group * nz), dma(group * nz), dma(3)],
         compiler_params=pltpu.CompilerParams(
             collective_id=0, has_side_effects=True, vmem_limit_bytes=63 * 1024 * 1024
         ),

time: 235 us -> 223 us (0.949)
  Pallas kernels: 229 us -> 218 us
    pallas_call x1, Pallas kernels: 229 us -> 218 us  [per_device(): pl.pallas_call(functools.partial(body, n_sp, n_tp, heads), out_shape=jax....]
where the time goes in v2:
time: 223 us
  Pallas kernels  218 us (98%)
  local copies, waits for them, and re-layouts  3.17 us (1%)
    pallas_call x1, Pallas kernels, per_device(): pl.pallas_call(functools.partial(body, n_sp, n_tp, heads), out_shape=jax....  218 us

profile of v2, /device:TPU:19, one launch (start us, length us, event | category | flops | bytes accessed | tf_op | source)
XLA Modules:
  0.0 222.5 jit_solution(3321368355109507515)
XLA Ops:
  0.0 1.3 pad.4.gate_ref
  1.3 1.9 pad_maximum_fusion.kv_ref
  3.1 217.5 %shard_map.91 = bf16[128,2048]{1,0:T(8,128)(2,1)} custom-call(bf16[512,256]{1,0:T(8,128)(2,1)} %q_ref.1, bf16[512,512]{1,0:T(8,128)(2,1)} %pad_maximum_fusion.kv_ref, f32[8,512]{1,0:T(8,128)} %pad.4.gate_ref, bf16[128,2048]{1,0:T(8,128)(2,1)} %res_ref.1, bf16[1024,2048]{1,0:T(8,128)(2,1)} %wout_hbm.1, f32[1,2048]{1,0:T(1,128)} %bitcast.2, ...), custom_call_target="tpu_custom_call" | custom-call | tf_op jit(solution)/shard_map/pallas_call | solution.py:371
  220.7 1.9 copy.11

commit v3 on v2

--- a/solution.py
+++ b/solution.py
@@ -17,9 +17,9 @@
     q_ref, kv_ref, gate_ref, res_ref, wout_hbm, gain_ref, wup_hbm, wdn_hbm,
     out_ref,
     kv_all, gate_all, m_s, l_s, acc_s, att, att_in, wout, rsum,
-    wu, wd, norm_all, hid, psend, precv,
+    wu, wd, norm_all, hid, psend, pmate, pcomb, precv,
     kv_s1, kv_s2, kv_r, g_s1, g_s2, g_r, u_s1, u_s2, u_r, d_s1, d_s2, d_r,
-    a_s, a_r, n_s, n_r, p_s, p_r, loc,
+    a_s, a_r, n_s, n_r, p_s, p_r, q_s, q_r, loc,
 ):
     ny = n_tp // 2
     nz = n_sp // ny
@@ -61,10 +61,16 @@
                             device_id_type=pl.DeviceIdType.MESH)
     pl.semaphore_wait(barrier, nz - 1 + ny - 1 + group - 1)
 
-    def kv_first(dz):
-        to = (z + dz) * ny + y
-        return (rcopy(kv_ref, kv_all.at[me], kv_s1.at[dz], kv_r.at[me], to),
-                rcopy(gate_ref, gate_all.at[me], g_s1.at[dz], g_r.at[me], to))
+    def kv_up(zs):
+        s = zs * ny + y
+        to = me + ny
+        return (rcopy(kv_all.at[s], kv_all.at[s], kv_s1.at[zs], kv_r.at[s], to),
+                rcopy(gate_all.at[s], gate_all.at[s], g_s1.at[zs], g_r.at[s], to))
+
+    def kv_first():
+        to = me + ny
+        return (rcopy(kv_ref, kv_all.at[me], kv_s1.at[z], kv_r.at[me], to),
+                rcopy(gate_ref, gate_all.at[me], g_s1.at[z], g_r.at[me], to))
 
     def kv_own(dy):
         to = z * ny + (y + dy) % ny
@@ -108,11 +114,10 @@
         s = zs * ny + y
         return rcopy(wd.at[s], wd.at[s], d_s2.at[zs * ny + dy], d_r.at[s], z * ny + (y + dy) % ny)
 
-    for dz in range(1, nz):
-        @pl.when(z + dz < nz)
-        def _(dz=dz):
-            for c in kv_first(dz):
-                c.start()
+    @pl.when(z + 1 < nz)
+    def _():
+        for c in kv_first():
+            c.start()
     for dy in range(1, ny):
         @pl.when((y + dy) % ny > y)
         def _(dy=dy):
@@ -125,9 +130,9 @@
     local_up.start()
     local_dn.start()
     for dz in range(1, nz):
-        up_first(dz).start()
-    for dy in range(1, ny):
-        up_own(dy).start()
+        @pl.when(z + dz >= nz)
+        def _(dz=dz):
+            up_first(dz).start()
 
     scale = hd ** (-0.5) * LOG2E
 
@@ -170,9 +175,23 @@
                 own = zs * ny + y
                 rcopy(kv_ref, kv_all.at[own], kv_s1.at[0], kv_r.at[own], me).wait_recv()
                 rcopy(gate_ref, gate_all.at[own], g_s1.at[0], g_r.at[own], me).wait_recv()
+
+                @pl.when(z + 1 < nz)
+                def _():
+                    for c in kv_up(zs):
+                        c.start()
                 for dy in range(1, ny):
                     for c in kv_forward(zs, dy):
                         c.start()
+
+            @pl.when(zs == 0)
+            def _():
+                for dz in range(1, nz):
+                    @pl.when(z + dz < nz)
+                    def _(dz=dz):
+                        up_first(dz).start()
+                for dy in range(1, ny):
+                    up_own(dy).start()
 
             def column(dy, carry):
                 s = zs * ny + (y + dy) % ny
@@ -215,8 +234,13 @@
     mean_square = jnp.mean(total * total, axis=-1, keepdims=True)
     normed = (total * lax.rsqrt(mean_square + 1e-06) * gain_ref[...]).astype(jnp.bfloat16)
 
+    chips = group // 2
+    core = tp % 2
+    mate = slot + 1 - 2 * core
+
     def block(ref, b):
-        return ref.at[pl.ds(pl.multiple_of(b * rows, rows), rows), :]
+        at = (b % 2) * chips + b // 2
+        return ref.at[pl.ds(pl.multiple_of(at * rows, rows), rows), :]
 
     block(norm_all, slot)[...] = normed
 
@@ -224,10 +248,6 @@
         zo, to = other // n_tp, other % n_tp
         return rcopy(block(norm_all, src), block(norm_all, src), n_s.at[sem], n_r.at[src],
                      (z - par + zo) * ny + y, to)
-
-    chips = group // 2
-    core = tp % 2
-    mate = slot + 1 - 2 * core
 
     def normed_chip(k):
         return normed_row(slot, k, (slot + 2 * k) % group)
@@ -283,24 +303,42 @@
     per = max(1, 128 // cs)
     span = ny * cs
 
-    def part(ref, b, zs):
-        return ref.at[pl.ds(pl.multiple_of(b * rows, rows), rows),
+    mine = slot // 2
+
+    def part(ref, at, count, zs):
+        return ref.at[pl.ds(pl.multiple_of(at * rows, rows), count * rows),
                       pl.ds(pl.multiple_of(zs * span, span), span)]
 
-    def partial_to(o, zs):
-        other, sp_to, tp_to = member(o)
-        return rcopy(part(psend, other, zs), part(precv, slot, zs), p_s.at[o * nz + zs],
-                     p_r.at[slot * nz + zs], sp_to, tp_to)
+    def to_mate(zs):
+        return rcopy(part(psend, (1 - core) * chips, chips, zs), part(pmate, 0, chips, zs),
+                     q_s.at[zs], q_r.at[zs], me, mate % n_tp)
+
+    def partial_to(k, zs):
+        chip = (mine + k) % chips
+        other = chip * 2 + core
+        return rcopy(part(pcomb, chip, 1, zs), part(precv, mine, 1, zs), p_s.at[k * nz + zs],
+                     p_r.at[mine * nz + zs], (z - par + other // n_tp) * ny + y, other % n_tp)
+
+    def level_of(dz):
+        return (z - dz + nz) % nz
 
     def down_level(dz):
-        zs = (z - dz + nz) % nz
+        zs = level_of(dz)
         for k in range(ny // per):
             ws = [wd[zs * ny + k * per + i] for i in range(per)]
             w = ws[0] if per == 1 else jnp.concatenate(ws, axis=1)
             cols = pl.ds(pl.multiple_of((zs * ny + k * per) * cs, per * cs), per * cs)
             psend[:, cols] = jnp.dot(hid[...], w, preferred_element_type=jnp.float32).astype(jnp.bfloat16)
-        for o in range(1, group):
-            partial_to(o, zs).start()
+        to_mate(zs).start()
+
+    def combine(dz):
+        zs = level_of(dz)
+        to_mate(zs).wait_recv()
+        both = (part(psend, core * chips, chips, zs)[...].astype(jnp.float32)
+                + part(pmate, 0, chips, zs)[...].astype(jnp.float32))
+        part(pcomb, 0, chips, zs)[...] = both.astype(jnp.bfloat16)
+        for k in range(1, chips):
+            partial_to(k, zs).start()
 
     local_dn.wait()
     for dz in range(nz):
@@ -311,19 +349,28 @@
             s = zs * ny + (y + dy) % ny
             rcopy(dn_half(0), wd.at[s], d_s1.at[0], d_r.at[s], me).wait_recv()
         down_level(dz)
-
-    total = rsum[...] + block(psend, slot)[...].astype(jnp.float32)
-    for o in range(1, group):
-        src = (slot + o) % group
+        if dz > 0:
+            combine(dz - 1)
+    combine(nz - 1)
+
+    total = rsum[...]
+    whole_row = lambda ref, at: ref[pl.ds(pl.multiple_of(at * rows, rows), rows), :].astype(jnp.float32)
+    total += whole_row(pcomb, mine)
+    for k in range(1, chips):
+        src = (mine + k) % chips
         for zs in range(nz):
-            rcopy(part(psend, src, zs), part(precv, src, zs), p_s.at[0], p_r.at[src * nz + zs], me).wait_recv()
-        total += block(precv, src)[...].astype(jnp.float32)
+            rcopy(part(pcomb, src, 1, zs), part(precv, src, 1, zs), p_s.at[0], p_r.at[src * nz + zs], me).wait_recv()
+        total += whole_row(precv, src)
     out_ref[...] = total.astype(jnp.bfloat16)
 
+    @pl.when(z + 1 < nz)
+    def _():
+        for c in kv_first():
+            c.wait_send()
     for dz in range(1, nz):
-        @pl.when(z + dz < nz)
+        @pl.when((z + 1 < nz) & (z - dz >= 0))
         def _(dz=dz):
-            for c in kv_first(dz):
+            for c in kv_up(z - dz):
                 c.wait_send()
         up_first(dz).wait_send()
         dn_first(dz).wait_send()
@@ -349,9 +396,10 @@
         normed_chip(k).wait_send()
     for k in range(chips):
         normed_mate(k).wait_send()
-    for o in range(1, group):
-        for zs in range(nz):
-            partial_to(o, zs).wait_send()
+    for zs in range(nz):
+        to_mate(zs).wait_send()
+        for k in range(1, chips):
+            partial_to(k, zs).wait_send()
 
 
 def per_device(n_sp, n_tp, queries, keys, values, cum_gate, residual, w_out, gain, w_up, w_down):
@@ -388,10 +436,12 @@
             pltpu.VMEM((group * rows, features), bf),
             pltpu.VMEM((group * rows, half), bf),
             pltpu.VMEM((group * rows, features), bf),
-            pltpu.VMEM((group * rows, features), bf),
+            pltpu.VMEM((n_tp * rows, features), bf),
+            pltpu.VMEM((n_tp * rows, features), bf),
+            pltpu.VMEM((n_tp * rows, features), bf),
         ]
         + [dma(nz), dma(n_sp), dma(n_sp)] * 4
-        + [dma(n_tp), dma(n_tp), dma(group), dma(group), dma(group * nz), dma(group * nz), dma(3)],
+        + [dma(n_tp), dma(n_tp), dma(group), dma(group), dma(group * nz), dma(group * nz), dma(nz), dma(nz), dma(3)],
         compiler_params=pltpu.CompilerParams(
             collective_id=0, has_side_effects=True, vmem_limit_bytes=63 * 1024 * 1024
         ),

time: 223 us -> 208 us (0.933)
  Pallas kernels: 218 us -> 202 us
    pallas_call x1, Pallas kernels: 218 us -> 202 us  [per_device(): pl.pallas_call(functools.partial(body, n_sp, n_tp, heads), out_shape=jax....]
where the time goes in v3:
time: 208 us; the launch traced here: 207 us
  Pallas kernels  202 us (97%)
  local copies, waits for them, and re-layouts  3.17 us (2%)
    pallas_call x1, Pallas kernels, per_device(): pl.pallas_call(functools.partial(body, n_sp, n_tp, heads), out_shape=jax....  202 us

profile of v3, /device:TPU:19, one launch (start us, length us, event | category | flops | bytes accessed | tf_op | source)
XLA Modules:
  0.0 206.6 jit_solution(2014937139795865965)
XLA Ops:
  0.0 1.3 pad.4.gate_ref
  1.3 1.9 pad_maximum_fusion.kv_ref
  3.1 201.5 %shard_map.91 = bf16[128,2048]{1,0:T(8,128)(2,1)} custom-call(bf16[512,256]{1,0:T(8,128)(2,1)} %q_ref.1, bf16[512,512]{1,0:T(8,128)(2,1)} %pad_maximum_fusion.kv_ref, f32[8,512]{1,0:T(8,128)} %pad.4.gate_ref, bf16[128,2048]{1,0:T(8,128)(2,1)} %res_ref.1, bf16[1024,2048]{1,0:T(8,128)(2,1)} %wout_hbm.1, f32[1,2048]{1,0:T(1,128)} %bitcast.2, ...), custom_call_target="tpu_custom_call" | custom-call | tf_op jit(solution)/shard_map/pallas_call | solution.py:419
  204.7 1.9 copy.11

commit v4 on v3

--- a/solution.py
+++ b/solution.py
@@ -133,6 +133,12 @@
         @pl.when(z + dz >= nz)
         def _(dz=dz):
             up_first(dz).start()
+    for dy in range(1, ny):
+        up_own(dy).start()
+    for dz in range(1, nz):
+        @pl.when((z + dz >= nz) & (par == 0))
+        def _(dz=dz):
+            dn_first(dz).start()
 
     scale = hd ** (-0.5) * LOG2E
 
@@ -190,8 +196,10 @@
                     @pl.when(z + dz < nz)
                     def _(dz=dz):
                         up_first(dz).start()
-                for dy in range(1, ny):
-                    up_own(dy).start()
+                for dz in range(1, nz):
+                    @pl.when((z + dz < nz) & (par == 1))
+                    def _(dz=dz):
+                        dn_first(dz).start()
 
             def column(dy, carry):
                 s = zs * ny + (y + dy) % ny
@@ -222,6 +230,15 @@
 
     for o in range(1, n_tp):
         heads_to(o).start()
+    for dz in range(1, nz):
+        zs = (z - dz + nz) % nz
+        s = zs * ny + y
+        rcopy(up_half(0), wu_at(s), u_s1.at[0], u_r.at[s], me).wait_recv()
+        for dy in range(1, ny):
+            up_forward(zs, dy).start()
+    for dy in range(1, ny):
+        dn_own(dy).start()
+
     att_in[pl.ds(tp, 1)] = att[pl.ds(tp, 1)]
     local_wout.wait()
     for o in range(1, n_tp):
@@ -259,16 +276,10 @@
         normed_chip(k).start()
     normed_mate(0).start()
     for dz in range(1, nz):
-        dn_first(dz).start()
-    for dy in range(1, ny):
-        dn_own(dy).start()
-
-    for dz in range(1, nz):
-        zs = (z - dz + nz) % nz
-        s = zs * ny + y
-        rcopy(up_half(0), wu_at(s), u_s1.at[0], u_r.at[s], me).wait_recv()
-        for dy in range(1, ny):
-            up_forward(zs, dy).start()
+        @pl.when((z + dz < nz) == (par == 0))
+        def _(dz=dz):
+            dn_first(dz).start()
+
     for k in range(1, chips):
         src = (slot + 2 * k) % group
         rcopy(block(norm_all, src), block(norm_all, src), n_s.at[0], n_r.at[src], me).wait_recv()

time: 208 us -> 199 us (0.957)
  Pallas kernels: 202 us -> 194 us
    pallas_call x1, Pallas kernels: 202 us -> 194 us  [per_device(): pl.pallas_call(functools.partial(body, n_sp, n_tp, heads), out_shape=jax....]
where the time goes in v4:
time: 199 us
  Pallas kernels  194 us (97%)
  local copies, waits for them, and re-layouts  3.17 us (2%)
    pallas_call x1, Pallas kernels, per_device(): pl.pallas_call(functools.partial(body, n_sp, n_tp, heads), out_shape=jax....  194 us

profile of v4, /device:TPU:19, one launch (start us, length us, event | category | flops | bytes accessed | tf_op | source)
XLA Modules:
  0.0 199.3 jit_solution(15531628317503406597)
XLA Ops:
  0.0 1.3 pad.4.gate_ref
  1.3 1.9 pad_maximum_fusion.kv_ref
  3.1 194.2 %shard_map.91 = bf16[128,2048]{1,0:T(8,128)(2,1)} custom-call(bf16[512,256]{1,0:T(8,128)(2,1)} %q_ref.1, bf16[512,512]{1,0:T(8,128)(2,1)} %pad_maximum_fusion.kv_ref, f32[8,512]{1,0:T(8,128)} %pad.4.gate_ref, bf16[128,2048]{1,0:T(8,128)(2,1)} %res_ref.1, bf16[1024,2048]{1,0:T(8,128)(2,1)} %wout_hbm.1, f32[1,2048]{1,0:T(1,128)} %bitcast.2, ...), custom_call_target="tpu_custom_call" | custom-call | tf_op jit(solution)/shard_map/pallas_call | solution.py:430
  197.4 1.9 copy.11
